TPU v7x, 32 devices: a whole 2x2x4 slice. The times are simulated.
32 devices in a mesh: ep: 16 (over z, y, core), tp: 2 (over x).
Axes of the slice: x: 2, y: 2, z: 4, core: 2. Of those that a mesh axis runs over, the one named last changes fastest.
Arguments:
- tokens: bfloat16 [256, 2048], P('ep'), may hold values from -6 to 6
- positions: int32 [256], P('ep'), may hold values from 1024 to 16383
- state: float32 [256, 4, 128, 128], P('ep', 'tp'), may hold values from -1 to 1
- mix_gain: float32 [2048], replicated, may hold values from 0.1 to 1.9
- w_query: bfloat16 [2048, 512], P(None, 'tp'), may hold values from -0.125 to 0.125
- w_key: bfloat16 [2048, 512], P(None, 'tp'), may hold values from -0.125 to 0.125
- w_value: bfloat16 [2048, 512], P(None, 'tp'), may hold values from -0.125 to 0.125
- w_out: bfloat16 [512, 2048], P('tp'), may hold values from -0.25 to 0.25
- ffn_gain: float32 [2048], replicated, may hold values from 0.1 to 1.9
- branch_gate: bfloat16 [2048], replicated, may hold values from -0.125 to 0.125
- dense_gate: bfloat16 [2048, 4096], P('tp', 'ep'), may hold values from -0.125 to 0.125
- dense_up: bfloat16 [2048, 4096], P('tp', 'ep'), may hold values from -0.125 to 0.125
- dense_down: bfloat16 [4096, 2048], P('ep', 'tp'), may hold values from -0.09375 to 0.09375
- routes: int32 [256, 6], P('ep'), may hold values from 0 to 15, all different within a row; in each aligned block of 16 rows (0 to 15, 16 to 31, ...) at most 12 rows name the same one
- route_scores: float32 [256, 6], P('ep'), may hold values from 0.05 to 1
- expert_gate: bfloat16 [16, 2048, 512], P('ep', None, 'tp'), may hold values from -0.125 to 0.125
- expert_up: bfloat16 [16, 2048, 512], P('ep', None, 'tp'), may hold values from -0.125 to 0.125
- expert_down: bfloat16 [16, 512, 2048], P('ep', 'tp'), may hold values from -0.25 to 0.25
Outputs:
- layer_out: bfloat16 [256, 2048], P('ep', 'tp')
Inputs may be any that keep to these rules, and one draw needn't show every extreme that they name: `routes`: each row names 6 different experts. In each aligned block of 16 rows (the rows of one index of ep) no expert is named by more than 12 rows, a bound that some block reaches.
All inputs are finite; a program needn't handle non-finite values.
Results may differ from a plain program's by a relative error of at most 0.012.
Values may be sent and summed in bfloat16 or wider, within the bound.
A program may use at most 64 MiB of HBM per device.

v0:
```python
import jax
import jax.numpy as jnp
from jax import lax
from jax.sharding import PartitionSpec as P

EPS = 1e-06


def normalize(inputs, scale_vec):
    values = inputs.astype(jnp.float32)
    return values * lax.rsqrt(jnp.mean(values * values, axis=-1, keepdims=True) + EPS) * scale_vec


def rotate(vectors, where):
    half = vectors.shape[-1] // 2
    inverse = 1.0 / 10000.0 ** jnp.linspace(0.0, 1.0, half, dtype=jnp.float32)
    angle = where.astype(jnp.float32)[:, None] * inverse[None, :]
    cosine = jnp.cos(angle)[:, None, :]
    sine = jnp.sin(angle)[:, None, :]
    first = vectors[..., :half]
    second = vectors[..., half:]
    return jnp.concatenate(
        [first * cosine - second * sine, second * cosine + first * sine], axis=-1
    )


def on_device(
    tokens,
    positions,
    state,
    mix_gain,
    w_query,
    w_key,
    w_value,
    w_out,
    ffn_gain,
    branch_gate,
    dense_gate,
    dense_up,
    dense_down,
    routes,
    route_scores,
    expert_gate,
    expert_up,
    expert_down,
):
    sequences = tokens.shape[0]
    model_width = tokens.shape[1]
    tp_count = lax.axis_size("tp")
    ep_count = lax.axis_size("ep")
    columns = model_width // tp_count
    tp_index = lax.axis_index("tp")
    local_heads = state.shape[1]
    head_dim = state.shape[2]
    normed = normalize(tokens, mix_gain).astype(jnp.bfloat16)
    query_vec = jnp.dot(normed, w_query, preferred_element_type=jnp.float32).reshape(
        sequences, local_heads, head_dim
    )
    key_vec = jnp.dot(normed, w_key, preferred_element_type=jnp.float32).reshape(
        sequences, local_heads, head_dim
    )
    value_vec = jnp.dot(normed, w_value, preferred_element_type=jnp.float32).reshape(
        sequences, local_heads, head_dim
    )
    query_vec = rotate(query_vec, positions)
    key_vec = rotate(key_vec, positions) * head_dim ** (-0.5)
    all_heads = local_heads * tp_count
    head_index = (tp_index * local_heads + jnp.arange(local_heads, dtype=jnp.int32)).astype(
        jnp.float32
    )
    decay_rate = 1.0 - 2.0 ** (-5.0 - 5.0 * head_index / (all_heads - 1))
    new_state = (
        decay_rate[None, :, None, None] * state + key_vec[:, :, :, None] * value_vec[:, :, None, :]
    )
    retrieved = jnp.einsum("bhd,bhde->bhe", query_vec, new_state, precision=lax.Precision.HIGHEST)
    retrieved = retrieved * lax.rsqrt(jnp.mean(retrieved * retrieved, axis=-1, keepdims=True) + EPS)
    retrieved = retrieved.reshape(sequences, local_heads * head_dim).astype(jnp.bfloat16)
    head_partial = jnp.dot(retrieved, w_out, preferred_element_type=jnp.float32).astype(
        jnp.bfloat16
    )
    mixer_out = lax.psum(head_partial.astype(jnp.float32).astype(jnp.bfloat16), "tp").astype(
        jnp.float32
    )
    after_mix = tokens.astype(jnp.float32) + mixer_out
    ffn_in = normalize(after_mix, ffn_gain).astype(jnp.bfloat16)
    own_cols = lax.dynamic_slice_in_dim(ffn_in, tp_index * columns, columns, 1)
    per_device = expert_gate.shape[0]
    experts = per_device * ep_count
    fanout = routes.shape[1]
    capacity = max(2, min(sequences, 2 * sequences * fanout // experts))
    slot_count = experts * capacity
    marks = (routes[:, :, None] == jnp.arange(experts, dtype=jnp.int32)[None, None, :]).astype(
        jnp.int32
    )
    flattened = marks.reshape(sequences * fanout, experts)
    ranking = jnp.sum((jnp.cumsum(flattened, axis=0) - flattened) * flattened, axis=1).reshape(
        sequences, fanout
    )
    slot_index = routes * capacity + ranking
    matches = jnp.arange(slot_count, dtype=jnp.int32)[:, None, None] == slot_index[None]
    placing = jnp.any(matches, axis=2).astype(jnp.bfloat16)
    route_weights = route_scores / jnp.sum(route_scores, axis=1, keepdims=True)
    combining = jnp.sum(jnp.where(matches, route_weights[None], 0.0), axis=2).T
    packed = jnp.dot(placing, own_cols, preferred_element_type=jnp.float32).astype(jnp.bfloat16)
    packed = packed.reshape(experts, capacity, own_cols.shape[1])
    received = lax.all_to_all(packed, "ep", split_axis=0, concat_axis=0, tiled=True)
    received = lax.all_gather(received, "tp", axis=2, tiled=True)
    count = received.shape[1]
    grouped = received.reshape(ep_count, per_device, count, model_width)
    gate_pre = jnp.einsum(
        "skcd,kdw->skcw", grouped, expert_gate, preferred_element_type=jnp.float32
    )
    up_pre = jnp.einsum("skcd,kdw->skcw", grouped, expert_up, preferred_element_type=jnp.float32)
    hidden = (jax.nn.silu(gate_pre) * up_pre).astype(jnp.bfloat16)
    partial_out = jnp.einsum(
        "skcw,kwd->skcd", hidden, expert_down, preferred_element_type=jnp.float32
    )
    blocks_out = partial_out.astype(jnp.bfloat16).reshape(
        ep_count, per_device, count, tp_count, columns
    )
    traded = lax.all_to_all(blocks_out, "tp", split_axis=3, concat_axis=3, tiled=True)
    mine = jnp.sum(traded.astype(jnp.float32), axis=3).astype(jnp.bfloat16)
    mine = mine.reshape(ep_count * per_device, count, columns)
    returned = lax.all_to_all(mine, "ep", split_axis=0, concat_axis=0, tiled=True)
    experts_out = jnp.dot(
        combining,
        returned.reshape(slot_count, columns).astype(jnp.float32),
        precision=lax.Precision.HIGHEST,
    )
    hidden_units = dense_gate.shape[1]
    both_weights = jnp.concatenate([dense_gate, dense_up], axis=1)
    pre_parts = jnp.dot(
        lax.all_gather(own_cols, "ep", axis=0, tiled=True),
        both_weights,
        preferred_element_type=jnp.float32,
    ).astype(jnp.bfloat16)
    pre_total = lax.psum(pre_parts.astype(jnp.float32).astype(jnp.bfloat16), "tp").astype(
        jnp.float32
    )
    dense_hidden = (jax.nn.silu(pre_total[:, :hidden_units]) * pre_total[:, hidden_units:]).astype(
        jnp.bfloat16
    )
    dense_out = lax.psum_scatter(
        jnp.dot(dense_hidden, dense_down, preferred_element_type=jnp.float32),
        "ep",
        scatter_dimension=0,
        tiled=True,
    )
    branch_weight = jax.nn.sigmoid(jnp.dot(ffn_in, branch_gate, preferred_element_type=jnp.float32))
    residual_cols = lax.dynamic_slice_in_dim(after_mix, tp_index * columns, columns, 1)
    layer_out = residual_cols + experts_out + branch_weight[:, None] * dense_out
    return layer_out.astype(jnp.bfloat16)


def solution(mesh):
    placed = (
        P("ep", None),
        P("ep"),
        P("ep", "tp", None, None),
        P(),
        P(None, "tp"),
        P(None, "tp"),
        P(None, "tp"),
        P("tp", None),
        P(),
        P(),
        P("tp", "ep"),
        P("tp", "ep"),
        P("ep", "tp"),
        P("ep", None),
        P("ep", None),
        P("ep", None, "tp"),
        P("ep", None, "tp"),
        P("ep", "tp", None),
    )
    return jax.shard_map(
        on_device, mesh=mesh, in_specs=placed, out_specs=P("ep", "tp"), check_vma=False
    )
```

profile of v0, /device:TPU:0, one launch (start us, length us, event | category | flops | bytes accessed | tf_op | source)
XLA Modules:
  0.0 169.2 jit_solution(17816289287856958037)
XLA Ops:
  6.5 0.0 copy-start
  6.5 0.0 all-reduce.3.cloned.1.call-start
  6.6 0.8 convert_element_type.77
  7.4 1.0 fusion.30
  8.5 1.6 fusion.47
  10.1 1.6 fusion.45
  11.6 0.0 copy-done.1
  11.7 0.0 copy-done.7
  11.7 1.5 fusion.49
  13.2 0.0 copy-start.3
  13.2 0.1 fusion.41
  13.3 0.1 multiply_cosine_fusion
  13.4 0.0 copy-start.10
  13.4 0.1 multiply_subtract_fusion
  13.5 0.1 pad_maximum_fusion
  13.7 2.1 %fusion = f32[16,2,1,128]{3,2,1,0:T(1,128)S(1)} fusion(f32[16,2,128,1]{2,3,1,0:T(1,128)S(1)} %bitcast.86, f32[16,2,128,128]{3,2,1,0:T(8,128)S(1)} %copy-done.2, f32[16,2,128]{2,1,0:T(2,128)S(1)} %mul.244, f32[16,2,128]{2,1,0:T(2,128)S(1)} %get-tuple-element.17, f32[2]{0:T(128)S(1)} %power_subtract_fusion), kind=kOutput, calls=%fused_computation.2 | convolution fusion | flops 7864320 | bytes 2162696 | tf_op jit(solution)/shard_map/bhd,bhde->bhe/dot_general | solution.py:75
  15.7 0.1 multiply_reduce_fusion.1
  15.8 0.1 multiply_convert_fusion.1
  15.9 0.9 convolution_convert_fusion.1
  16.8 0.0 all-reduce.3.cloned.1.call-update
  16.9 0.1 copy.59
  16.9 0.1 eq.30
  17.0 0.1 fusion.38
  17.1 0.1 reduce_window_sum.11
  17.3 0.2 select_reduce_fusion.1
  17.4 0.1 reshape.154
  17.5 0.1 copy.60
  17.6 0.1 fusion.37
  17.7 23.0 %all-reduce.3.cloned.1.call-done = bf16[16,2048]{1,0:T(8,128)(2,1)} async-done(((bf16[16,2048]{1,0:T(8,128)(2,1)}), bf16[16,2048]{1,0:T(8,128)(2,1)}) %all-reduce.3.cloned.1.call-update) | async-done | bytes 65552 | tf_op jit(solution)/shard_map/psum | solution.py:81
  40.7 1.6 convert_add_fusion
  42.3 0.9 multiply_convert_fusion
  43.3 22.9 %all_gather.7 = bf16[256,1024]{1,0:T(8,128)(2,1)S(1)} all-gather(bf16[16,1024]{1,0:T(8,128)(2,1)S(1)} %constant_dynamic-slice_fusion), channel_id=1, replica_groups=mesh['ep'=16,'tp'=2] {'ep'}, dimensions={0}, use_global_device_ids=true | all-gather | bytes 557056 | tf_op jit(solution)/shard_map/all_gather | solution.py:133
  66.2 0.3 convolution_convert_fusion.2
  66.5 0.9 reshape.155
  67.4 3.6 %all-to-all-start = ((bf16[16,12,1024]{2,1,0:T(8,128)(2,1)}), bf16[16,12,1024]{2,1,0:T(8,128)(2,1)S(1)}, u32[]{:S(2)}, u32[]{:S(2)}) async-start(bf16[16,12,1024]{2,1,0:T(8,128)(2,1)} %reshape.155), calls=%async_computation | async-start | bytes 1048576 | tf_op jit(solution)/shard_map/all_to_all | solution.py:106
  70.9 0.0 copy-start.5
  71.0 0.0 all-reduce.5.cloned.1.call-start
  71.0 0.0 copy-done.12
  71.0 2.2 %convolution_convert_fusion.3 = bf16[256,512]{1,0:T(8,128)(2,1)} fusion(bf16[256,1024]{1,0:T(8,128)(2,1)S(1)} %all_gather.7, bf16[1024,256]{1,0:T(8,128)(2,1)S(1)} %copy-done.12, bf16[1024,256]{1,0:T(8,128)(2,1)} %param.30), kind=kOutput, calls=%fused_computation.7 | convolution fusion | flops 270663680 | bytes 1835008 | tf_op jit(solution)/shard_map/dot_general | solution.py:132
  73.2 0.0 all-reduce.5.cloned.1.call-update
  73.3 0.0 reduce-scatter.2.cloned.1.call-start
  73.3 24.4 %all-reduce.5.cloned.1.call-done = bf16[256,512]{1,0:T(8,128)(2,1)} async-done(((bf16[256,512]{1,0:T(8,128)(2,1)}), bf16[256,512]{1,0:T(8,128)(2,1)}) %all-reduce.5.cloned.1.call-update) | async-done | bytes 262160 | tf_op jit(solution)/shard_map/psum | solution.py:137
  97.7 1.0 convert_element_type.92
  98.8 0.0 copy-start.4
  98.8 1.3 fusion.33
  100.1 0.0 reduce-scatter.2.cloned.1.call-update
  100.1 0.0 all-to-all-done
  100.1 0.2 copy.61
  100.3 11.0 %all_gather.6 = bf16[16,12,2048]{2,0,1:T(8,128)(2,1)S(1)} all-gather(bf16[16,12,1024]{2,0,1:T(8,128)(2,1)S(1)} %copy.61), channel_id=1, replica_groups=mesh['ep'=16,'tp'=2] {'tp'}, dimensions={2}, use_global_device_ids=true | all-gather | bytes 1179648 | tf_op jit(solution)/shard_map/all_gather | solution.py:107
  111.4 1.1 convolution_bitcast_fusion.1
  112.4 2.3 %convolution_convert_fusion = bf16[16,12,2048]{2,0,1:T(8,128)(2,1)S(1)} fusion(bf16[1,256,2048]{2,1,0:T(8,128)(2,1)S(1)} %copy-done, bf16[16,12,2048]{2,0,1:T(8,128)(2,1)S(1)} %all_gather.6, bf16[1,2048,256]{2,1,0:T(8,128)(2,1)} %param.36, f32[16,1,12,256]{3,0,2,1:T(8,128)} %convolution_bitcast_fusion.1), kind=kOutput, calls=%fused_computation | convolution fusion | flops 403341312 | bytes 3866624 | tf_op jit(solution)/shard_map/skcw,kwd->skcd/dot_general | solution.py:115
  114.7 0.1 copy.77
  114.8 0.0 copy-start.11
  114.8 0.0 copy-start.9
  114.8 12.1 %all_to_all.15 = bf16[16,1,12,2,1024]{4,0,2,1,3:T(8,128)(2,1)S(1)} all-to-all(bf16[16,1,12,2,1024]{4,0,2,1,3:T(8,128)(2,1)S(1)} %bitcast.82), channel_id=1, replica_groups=mesh['ep'=16,'tp'=2] {'tp'}, dimensions={3} | all-to-all | bytes 1572864 | tf_op jit(solution)/shard_map/all_to_all | solution.py:121
  126.9 0.2 reduce_sum.72
  127.1 1.0 copy.64
  128.2 5.6 %all-to-all-start.2 = ((bf16[16,12,1024]{2,1,0:T(8,128)(2,1)}), bf16[16,12,1024]{2,1,0:T(8,128)(2,1)S(1)}, u32[]{:S(2)}, u32[]{:S(2)}) async-start(bf16[16,12,1024]{2,1,0:T(8,128)(2,1)} %copy.64), calls=%async_computation.2 | async-start | bytes 1048576 | tf_op jit(solution)/shard_map/all_to_all | solution.py:124
  133.9 0.1 select_reduce_fusion
  134.0 0.1 fusion.12
  134.1 14.8 %all-to-all-done.2 = bf16[16,12,1024]{2,1,0:T(8,128)(2,1)S(1)} async-done(((bf16[16,12,1024]{2,1,0:T(8,128)(2,1)}), bf16[16,12,1024]{2,1,0:T(8,128)(2,1)S(1)}, u32[]{:S(2)}, u32[]{:S(2)}) %all-to-all-start.2) | async-done | bytes 393248 | tf_op jit(solution)/shard_map/all_to_all | solution.py:124
  148.9 0.1 reshape.161
  149.0 11.9 %reduce-scatter.2.cloned.1.call-done = f32[16,1024]{1,0:T(8,128)} async-done(((f32[256,1024]{1,0:T(8,128)}), f32[16,1024]{1,0:T(8,128)}) %reduce-scatter.2.cloned.1.call-update) | async-done | bytes 65552 | tf_op jit(solution)/shard_map/reduce_scatter | solution.py:143
  160.9 1.7 %fusion.8 = bf16[16,1024]{1,0:T(8,128)(2,1)} fusion(f32[192,16]{0,1:T(8,128)S(1)} %select_reduce_fusion, bf16[192,1024]{1,0:T(8,128)(2,1)S(1)} %reshape.161, f32[16,1024]{1,0:T(8,128)} %reduce-scatter.2.cloned.1.call-done, f32[16,2048]{1,0:T(8,128)S(1)} %copy-done.6, s32[]{:T(128)S(6)} %select_n.8, f32[16]{0:T(128)S(1)} %fusion.12), kind=kOutput, calls=%fused_computation.15 | convolution fusion | flops 37814272 | bytes 569412 | tf_op jit(solution)/shard_map/dot_general | solution.py:125
  (29 shorter events, 0.2 us)
Async XLA Ops:
  6.5 105.9 %copy-start = (bf16[1,256,2048]{2,1,0:T(8,128)(2,1)S(1)}, bf16[1,256,2048]{2,1,0:T(8,128)(2,1)}, u32[]{:S(2)}) copy-start(bf16[1,256,2048]{2,1,0:T(8,128)(2,1)} %param.37) | copy-start | bytes 3145732
  6.5 5.1 %copy-start.1 = (bf16[16,2048]{1,0:T(8,128)(2,1)S(1)}, bf16[16,2048]{1,0:T(8,128)(2,1)}, u32[]{:S(2)}) copy-start(bf16[16,2048]{1,0:T(8,128)(2,1)} %param.20) | copy-start | bytes 196612
  6.5 5.1 %copy-start.7 = (f32[2048]{0:T(1024)S(1)}, f32[2048]{0:T(1024)}, u32[]{:S(2)}) copy-start(f32[2048]{0:T(1024)} %param.23) | copy-start | bytes 24580
  6.5 7.1 %copy-start.2 = (f32[16,2,128,128]{3,2,1,0:T(8,128)S(1)}, f32[16,2,128,128]{3,2,1,0:T(8,128)}, u32[]{:S(2)}) copy-start(f32[16,2,128,128]{3,2,1,0:T(8,128)} %param.22) | copy-start | bytes 6291460
  6.5 34.1 %all-reduce.3.cloned.1.call-start = ((), (), s32[]{:S(2)}) async-start(), calls=%async_computation.4 | async-start | bytes 131072 | tf_op jit(solution)/shard_map/psum | solution.py:81
  13.2 3.7 %copy-start.8 = (s32[16,6]{0,1:T(8,128)S(1)}, s32[16,6]{0,1:T(8,128)}, u32[]{:S(2)}) copy-start(s32[16,6]{0,1:T(8,128)} %param.33) | copy-start | bytes 1156
  13.2 2.7 %copy-start.3 = (bf16[256,2048]{1,0:T(8,128)(2,1)S(1)}, bf16[256,2048]{1,0:T(8,128)(2,1)}, u32[]{:S(2)}) copy-start(bf16[256,2048]{1,0:T(8,128)(2,1)} %param.27) | copy-start | bytes 3145732
  13.4 28.9 %copy-start.10 = (f32[2048]{0:T(1024)S(1)}, f32[2048]{0:T(1024)}, u32[]{:S(2)}) copy-start(f32[2048]{0:T(1024)} %param.28) | copy-start | bytes 24580
  16.8 54.2 %copy-start.12 = (bf16[1024,256]{1,0:T(8,128)(2,1)S(1)}, bf16[1024,256]{1,0:T(8,128)(2,1)}, u32[]{:S(2)}) copy-start(bf16[1024,256]{1,0:T(8,128)(2,1)} %param.31) | copy-start | bytes 1572868
  67.4 32.7 %all-to-all-start = ((bf16[16,12,1024]{2,1,0:T(8,128)(2,1)}), bf16[16,12,1024]{2,1,0:T(8,128)(2,1)S(1)}, u32[]{:S(2)}, u32[]{:S(2)}) async-start(bf16[16,12,1024]{2,1,0:T(8,128)(2,1)} %reshape.155), calls=%async_computation | async-start | bytes 1048576 | tf_op jit(solution)/shard_map/all_to_all | solution.py:106
  70.9 27.8 %copy-start.5 = (bf16[256,1024]{1,0:T(8,128)(2,1)S(1)}, bf16[256,1024]{1,0:T(8,128)(2,1)}, u32[]{:S(2)}) copy-start(bf16[256,1024]{1,0:T(8,128)(2,1)} %param.32) | copy-start | bytes 1572868
  71.0 26.8 %all-reduce.5.cloned.1.call-start = ((), (), s32[]{:S(2)}) async-start(), calls=%async_computation.5 | async-start | bytes 524288 | tf_op jit(solution)/shard_map/psum | solution.py:137
  73.3 87.6 %reduce-scatter.2.cloned.1.call-start = ((), (), s32[]{:S(2)}) async-start(), calls=%async_computation.6 | async-start | bytes 1114112 | tf_op jit(solution)/shard_map/reduce_scatter | solution.py:143
  98.8 12.6 %copy-start.4 = (bf16[1,2048,256]{2,1,0:T(8,128)(2,1)S(1)}, bf16[1,2048,256]{2,1,0:T(8,128)(2,1)}, u32[]{:S(2)}) copy-start(bf16[1,2048,256]{2,1,0:T(8,128)(2,1)} %param.35) | copy-start | bytes 3145732
  114.8 19.0 %copy-start.11 = (bf16[2048]{0:T(1024)(128)(2,1)S(1)}, bf16[2048]{0:T(1024)(128)(2,1)}, u32[]{:S(2)}) copy-start(bf16[2048]{0:T(1024)(128)(2,1)} %param.29) | copy-start | bytes 12292
  114.8 19.0 %copy-start.9 = (f32[16,6]{0,1:T(8,128)S(1)}, f32[16,6]{0,1:T(8,128)}, u32[]{:S(2)}) copy-start(f32[16,6]{0,1:T(8,128)} %param.34) | copy-start | bytes 1156
  126.9 34.0 %copy-start.6 = (f32[16,2048]{1,0:T(8,128)S(1)}, f32[16,2048]{1,0:T(8,128)}, u32[]{:S(2)}) copy-start(f32[16,2048]{1,0:T(8,128)} %get-tuple-element.6) | copy-start | bytes 393220
  128.2 20.7 %all-to-all-start.2 = ((bf16[16,12,1024]{2,1,0:T(8,128)(2,1)}), bf16[16,12,1024]{2,1,0:T(8,128)(2,1)S(1)}, u32[]{:S(2)}, u32[]{:S(2)}) async-start(bf16[16,12,1024]{2,1,0:T(8,128)(2,1)} %copy.64), calls=%async_computation.2 | async-start | bytes 1048576 | tf_op jit(solution)/shard_map/all_to_all | solution.py:124
Sparse Core Ops, SparseCore 0:
  17.0 23.6 all-reduce.2
  74.0 23.6 all-reduce.4
  101.4 59.4 reduce-scatter.1
where the time goes:
time: 170 us; the launch traced here: 169 us
  waiting for transfers between devices  74.1 us (44%)
  blocking collectives  46 us (27%)
  matrix products  16.6 us (10%)
  between operations  13.5 us (8%)
  starting transfers between devices  9.31 us (5%)
  other arithmetic  6.78 us (4%)
  local copies, waits for them, and re-layouts  2.79 us (2%)
    psum x1, waiting for transfers between devices, on_device(): lax.psum(pre_parts.astype(jnp.float32).astype(jnp.bfloat16), 'tp')  24.4 us
    psum x1, waiting for transfers between devices, on_device(): lax.psum(head_partial.astype(jnp.float32).astype(jnp.bfloat16), 'tp')  23 us
    all_gather x1, blocking collectives, on_device(): lax.all_gather(own_cols, 'ep', axis=0, tiled=True)  22.9 us
    all_to_all x1, waiting for transfers between devices, on_device(): lax.all_to_all(mine, 'ep', split_axis=0, concat_axis=0, tiled=True)  14.8 us
    all_to_all x1, blocking collectives, on_device(): lax.all_to_all(blocks_out, 'tp', split_axis=3, concat_axis=3, tiled=True)  12.1 us
    reduce_scatter x1, waiting for transfers between devices, on_device(): lax.psum_scatter(jnp.dot(dense_hidden, dense_down, preferred_element_type...  11.9 us
    all_gather x1, blocking collectives, on_device(): received = lax.all_gather(received, 'tp', axis=2, tiled=True)  11 us
    all_to_all x1, starting transfers between devices, on_device(): lax.all_to_all(mine, 'ep', split_axis=0, concat_axis=0, tiled=True)  5.62 us
  transfers between devices with their start and end apart: 5, of which 4 were waited for; matrix products, arithmetic and copies ran while one was open for 6% of the time, Pallas kernels for 0%

commit v1 on v0

v1 whole, which is shorter than its diff:
```python
import functools

import jax
import jax.numpy as jnp
from jax import lax
from jax.experimental import pallas as pl
from jax.experimental.pallas import tpu as pltpu
from jax.sharding import PartitionSpec as P

EPS = 1e-06
MESH = pl.DeviceIdType.MESH
F32 = jnp.float32
BF16 = jnp.bfloat16


def normalize(inputs, scale_vec):
    values = inputs.astype(jnp.float32)
    return values * lax.rsqrt(jnp.mean(values * values, axis=-1, keepdims=True) + EPS) * scale_vec


def rotate(vectors, where):
    half = vectors.shape[-1] // 2
    inverse = 1.0 / 10000.0 ** jnp.linspace(0.0, 1.0, half, dtype=jnp.float32)
    angle = where.astype(jnp.float32)[:, None] * inverse[None, :]
    cosine = jnp.cos(angle)[:, None, :]
    sine = jnp.sin(angle)[:, None, :]
    first = vectors[..., :half]
    second = vectors[..., half:]
    return jnp.concatenate(
        [first * cosine - second * sine, second * cosine + first * sine], axis=-1
    )


def split_ep(count):
    inner = 2 if count % 2 == 0 else 1
    rest = count // inner
    middle = 1
    while middle * middle * 4 <= rest and rest % (middle * 2) == 0:
        middle *= 2
    return rest // middle, middle, inner


class Dims:
    pass


def silu(v):
    return v / (1.0 + jnp.exp(-v))


def layer_kernel(n, *refs):
    (tok, hp, side, gain, bgate, eg_h, eu_h, ed_h, dg_h, du_h, dd_h, out,
     eg, eu, ed, dg, du, dd, hpr, am, g, pg, pu, s0, rc, s1, rx, s2, ry, s3, rz,
     w_sem, hp_s, hp_r, ag_s, ag_r, pg_s, pg_r, pu_s, pu_r,
     c_s, c_r, x_s, x_r, y_s, y_r, z_s, z_r) = refs
    A, B, C, T, R, D = n.A, n.B, n.C, n.T, n.R, n.D
    cols, L, NC = n.cols, n.L, n.NC
    cw = cols // NC
    rows = A * B * C * R
    ep = lax.axis_index("ep")
    t = lax.axis_index("tp")
    c = lax.rem(ep, C)
    b = lax.rem(lax.div(ep, C), B)
    a = lax.div(ep, B * C)

    def dev(a_, b_, c_):
        return {"ep": (a_ * B + b_) * C + c_}

    def add(i, d, m):
        return lax.rem(i + d, m)

    def slot(a_, b_, c_):
        return (c_ * B + b_) * A + a_

    def rws(s, count=1):
        return pl.ds(pl.multiple_of(s * R, R), count * R)

    loads = [pltpu.make_async_copy(src, dst, w_sem.at[i]) for i, (src, dst) in enumerate(
        ((dg_h, dg), (du_h, du), (eg_h, eg), (eu_h, eu), (ed_h, ed), (dd_h, dd)))]
    for load in loads:
        load.start()

    bar = pltpu.get_barrier_semaphore()
    peers = [dev(add(a, d, A), b, c) for d in range(1, A)]
    peers += [dev(a, add(b, d, B), c) for d in range(1, B)]
    peers += [dev(a, b, add(c, d, C)) for d in range(1, C)]
    peers += [{"tp": add(t, d, T)} for d in range(1, T)]
    for peer in peers:
        pl.semaphore_signal(bar, inc=1, device_id=peer, device_id_type=MESH)
    pl.semaphore_wait(bar, len(peers))

    sent = []

    def push(src, dst, ss, rs, where):
        copy = pltpu.make_async_remote_copy(
            src_ref=src, dst_ref=dst, send_sem=ss, recv_sem=rs, device_id=where, device_id_type=MESH
        )
        copy.start()
        sent.append(copy)

    def arrived(dst, rs):
        pltpu.make_async_remote_copy(
            src_ref=dst, dst_ref=dst, send_sem=rs, recv_sem=rs, device_id={"tp": t}, device_id_type=MESH
        ).wait_recv()

    for d in range(1, T):
        push(hp, hpr.at[d - 1], hp_s.at[d - 1], hp_r.at[d - 1], {"tp": add(t, d, T)})
    mixed = hp[...].astype(F32)
    for d in range(1, T):
        arrived(hpr.at[d - 1], hp_r.at[d - 1])
        mixed = mixed + hpr[d - 1].astype(F32)
    after = tok[...].astype(F32) + mixed
    am[...] = after
    ffn = (after * lax.rsqrt(jnp.mean(after * after, axis=-1, keepdims=True) + EPS) * gain[...]).astype(BF16)
    score = jnp.sum(ffn.astype(F32) * bgate[...].astype(F32), axis=-1, keepdims=True)
    branch = 1.0 / (1.0 + jnp.exp(-score))
    lane = lax.broadcasted_iota(jnp.int32, (R, L), 1)
    sides = jnp.where(lane == n.E, branch, side[...])
    high = sides.astype(BF16)
    low = (sides - high.astype(F32)).astype(BF16)
    mine = rws(slot(a, b, c))
    g[mine, 0:D] = ffn
    g[mine, D:D + L] = high
    g[mine, D + L:D + 2 * L] = low

    count = 0
    for da in range(1, A):
        push(g.at[mine], g.at[mine], ag_s.at[count], ag_r.at[slot(a, b, c)], dev(add(a, da, A), b, c))
        count += 1
    for da in range(A):
        aa = add(a, da, A)
        own = rws(slot(aa, b, c))
        if da > 0:
            arrived(g.at[own], ag_r.at[slot(aa, b, c)])
        for db in range(1, B):
            push(g.at[own], g.at[own], ag_s.at[count], ag_r.at[slot(aa, b, c)], dev(a, add(b, db, B), c))
            count += 1
        for dc in range(1, C):
            push(g.at[own], g.at[own], ag_s.at[count], ag_r.at[slot(aa, b, c)], dev(a, b, add(c, dc, C)))
            count += 1
    for da in range(A):
        aa = add(a, da, A)
        for db in range(1, B):
            bb = add(b, db, B)
            own = rws(slot(aa, bb, c))
            arrived(g.at[own], ag_r.at[slot(aa, bb, c)])
            for dc in range(1, C):
                push(g.at[own], g.at[own], ag_s.at[count], ag_r.at[slot(aa, bb, c)], dev(a, b, add(c, dc, C)))
                count += 1
    for dc in range(1, C):
        cc = add(c, dc, C)
        for da in range(A):
            for db in range(B):
                ss = slot(add(a, da, A), add(b, db, B), cc)
                arrived(g.at[rws(ss)], ag_r.at[ss])

    loads[0].wait()
    loads[1].wait()
    tile = min(rows, 256)
    own_cols = pl.ds(pl.multiple_of(t * cols, 128), cols)
    for r in range(0, rows, tile):
        xo = g[r:r + tile, own_cols]
        pg[0, r:r + tile, :] = jnp.dot(xo, dg[...], preferred_element_type=F32).astype(BF16)
        pu[0, r:r + tile, :] = jnp.dot(xo, du[...], preferred_element_type=F32).astype(BF16)
    for d in range(1, T):
        push(pg.at[0], pg.at[d], pg_s.at[d - 1], pg_r.at[d - 1], {"tp": add(t, d, T)})
        push(pu.at[0], pu.at[d], pu_s.at[d - 1], pu_r.at[d - 1], {"tp": add(t, d, T)})

    loads[2].wait()
    loads[3].wait()
    K = n.K
    hid, wgt, brw = {}, {}, {}
    for r in range(0, rows, tile):
        lanes = lax.broadcasted_iota(jnp.int32, (tile, L), 1)
        sd = g[r:r + tile, D:D + L].astype(F32) + g[r:r + tile, D + L:D + 2 * L].astype(F32)
        brw[r] = jnp.sum(jnp.where(lanes == n.E, sd, 0.0), axis=1, keepdims=True)
        for k in range(K):
            x = g[r:r + tile, 0:D]
            gate = jnp.dot(x, eg[k], preferred_element_type=F32)
            up = jnp.dot(x, eu[k], preferred_element_type=F32)
            hid[r, k] = (silu(gate) * up).astype(BF16)
            wgt[r, k] = jnp.sum(jnp.where(lanes == ep * K + k, sd, 0.0), axis=1, keepdims=True)
    loads[4].wait()
    loads[5].wait()

    for d in range(1, T):
        arrived(pg.at[d], pg_r.at[d - 1])
        arrived(pu.at[d], pu_r.at[d - 1])
    dense = {}
    for r in range(0, rows, tile):
        pre_g = pg[0, r:r + tile, :].astype(F32)
        pre_u = pu[0, r:r + tile, :].astype(F32)
        for d in range(1, T):
            pre_g = pre_g + pg[d, r:r + tile, :].astype(F32)
            pre_u = pre_u + pu[d, r:r + tile, :].astype(F32)
        dense[r] = (silu(pre_g) * pre_u).astype(BF16)

    per_c, per_b = A * B, A
    def chunk(k):
        return slice(k * cw, (k + 1) * cw)

    def stage0(k):
        for dt in range(T):
            start = pl.multiple_of(add(t, dt, T) * cols + k * cw, 128)
            for r in range(0, rows, tile):
                total = jnp.zeros((tile, cw), F32)
                for e in range(K):
                    total = total + wgt[r, e] * jnp.dot(hid[r, e], ed[e, :, pl.ds(start, cw)], preferred_element_type=F32)
                if dt == 0:
                    total = total + brw[r] * jnp.dot(dense[r], dd[:, chunk(k)], preferred_element_type=F32)
                s0[dt, r:r + tile, chunk(k)] = total.astype(BF16)
            for dc in range(1, C):
                cc = add(c, dc, C)
                i = (k * T + dt) * (C - 1) + dc - 1
                push(s0.at[dt, rws(cc * per_c, per_c), chunk(k)], rc.at[dc - 1, dt, :, chunk(k)],
                     c_s.at[i], c_r.at[i], dev(a, b, cc))

    def stage1(k):
        for dt in list(range(1, T)) + [0]:
            acc = s0[dt, rws(c * per_c, per_c), chunk(k)].astype(F32)
            for dc in range(1, C):
                i = (k * T + dt) * (C - 1) + dc - 1
                arrived(rc.at[dc - 1, dt, :, chunk(k)], c_r.at[i])
                acc = acc + rc[dc - 1, dt, :, chunk(k)].astype(F32)
            s1[dt, :, chunk(k)] = acc.astype(BF16)
            if dt > 0:
                i = k * (T - 1) + dt - 1
                push(s1.at[dt, :, chunk(k)], rx.at[dt - 1, :, chunk(k)], x_s.at[i], x_r.at[i], {"tp": add(t, dt, T)})

    def stage2(k):
        acc = s1[0, :, chunk(k)].astype(F32)
        for dt in range(1, T):
            i = k * (T - 1) + dt - 1
            arrived(rx.at[dt - 1, :, chunk(k)], x_r.at[i])
            acc = acc + rx[dt - 1, :, chunk(k)].astype(F32)
        s2[:, chunk(k)] = acc.astype(BF16)
        for db in range(1, B):
            bb = add(b, db, B)
            i = k * (B - 1) + db - 1
            push(s2.at[rws(bb * per_b, per_b), chunk(k)], ry.at[db - 1, :, chunk(k)], y_s.at[i], y_r.at[i], dev(a, bb, c))

    def stage3(k):
        acc = s2[rws(b * per_b, per_b), chunk(k)].astype(F32)
        for db in range(1, B):
            i = k * (B - 1) + db - 1
            arrived(ry.at[db - 1, :, chunk(k)], y_r.at[i])
            acc = acc + ry[db - 1, :, chunk(k)].astype(F32)
        s3[:, chunk(k)] = acc.astype(BF16)
        for da in range(1, A):
            aa = add(a, da, A)
            i = k * (A - 1) + da - 1
            push(s3.at[rws(aa), chunk(k)], rz.at[da - 1, :, chunk(k)], z_s.at[i], z_r.at[i], dev(aa, b, c))

    def stage4(k):
        acc = s3[rws(a), chunk(k)].astype(F32)
        for da in range(1, A):
            i = k * (A - 1) + da - 1
            arrived(rz.at[da - 1, :, chunk(k)], z_r.at[i])
            acc = acc + rz[da - 1, :, chunk(k)].astype(F32)
        base = am[:, pl.ds(pl.multiple_of(t * cols + k * cw, 128), cw)]
        out[:, chunk(k)] = (base + acc).astype(BF16)

    stages = (stage0, stage1, stage2, stage3, stage4)
    for step in range(NC + len(stages) - 1):
        for s, stage in enumerate(stages):
            if 0 <= step - s < NC:
                stage(step - s)

    for copy in sent:
        copy.wait_send()


def on_device(
    tokens,
    positions,
    state,
    mix_gain,
    w_query,
    w_key,
    w_value,
    w_out,
    ffn_gain,
    branch_gate,
    dense_gate,
    dense_up,
    dense_down,
    routes,
    route_scores,
    expert_gate,
    expert_up,
    expert_down,
):
    sequences = tokens.shape[0]
    model_width = tokens.shape[1]
    tp_count = lax.axis_size("tp")
    ep_count = lax.axis_size("ep")
    columns = model_width // tp_count
    tp_index = lax.axis_index("tp")
    local_heads = state.shape[1]
    head_dim = state.shape[2]
    normed = normalize(tokens, mix_gain).astype(jnp.bfloat16)
    query_vec = jnp.dot(normed, w_query, preferred_element_type=jnp.float32).reshape(
        sequences, local_heads, head_dim
    )
    key_vec = jnp.dot(normed, w_key, preferred_element_type=jnp.float32).reshape(
        sequences, local_heads, head_dim
    )
    value_vec = jnp.dot(normed, w_value, preferred_element_type=jnp.float32).reshape(
        sequences, local_heads, head_dim
    )
    query_vec = rotate(query_vec, positions)
    key_vec = rotate(key_vec, positions) * head_dim ** (-0.5)
    all_heads = local_heads * tp_count
    head_index = (tp_index * local_heads + jnp.arange(local_heads, dtype=jnp.int32)).astype(
        jnp.float32
    )
    decay_rate = 1.0 - 2.0 ** (-5.0 - 5.0 * head_index / (all_heads - 1))
    old = jnp.sum(query_vec[:, :, :, None] * state, axis=2)
    inner = jnp.sum(query_vec * key_vec, axis=2, keepdims=True)
    retrieved = decay_rate[None, :, None] * old + inner * value_vec
    retrieved = retrieved * lax.rsqrt(jnp.mean(retrieved * retrieved, axis=-1, keepdims=True) + EPS)
    retrieved = retrieved.reshape(sequences, local_heads * head_dim).astype(jnp.bfloat16)
    head_partial = jnp.dot(retrieved, w_out, preferred_element_type=jnp.float32).astype(
        jnp.bfloat16
    )

    n = Dims()
    n.A, n.B, n.C = split_ep(ep_count)
    n.T, n.R, n.D, n.cols = tp_count, sequences, model_width, columns
    n.K = expert_gate.shape[0]
    n.E = n.K * ep_count
    n.L = -(-(n.E + 1) // 128) * 128
    n.NC = 2 if columns % 256 == 0 else 1
    route_weights = route_scores / jnp.sum(route_scores, axis=1, keepdims=True)
    marks = routes[:, :, None] == jnp.arange(n.L, dtype=jnp.int32)[None, None, :]
    side = jnp.sum(jnp.where(marks, route_weights[:, :, None], 0.0), axis=1)

    A, B, C, T, R, D, NC = n.A, n.B, n.C, n.T, n.R, n.D, n.NC
    rows = ep_count * R
    hidden = dense_gate.shape[1]
    vm = pl.BlockSpec(memory_space=pltpu.VMEM)
    hbm = pl.BlockSpec(memory_space=pl.ANY)
    dma = pltpu.SemaphoreType.DMA
    vmem = pltpu.VMEM
    part = A * B * R
    scratch = [
        vmem(expert_gate.shape, BF16), vmem(expert_up.shape, BF16), vmem(expert_down.shape, BF16),
        vmem(dense_gate.shape, BF16), vmem(dense_up.shape, BF16), vmem(dense_down.shape, BF16),
        vmem((max(1, T - 1), R, D), BF16), vmem((R, D), F32),
        vmem((rows, D + 2 * n.L), BF16),
        vmem((T, rows, hidden), BF16), vmem((T, rows, hidden), BF16),
        vmem((T, rows, columns), BF16), vmem((max(1, C - 1), T, part, columns), BF16),
        vmem((T, part, columns), BF16), vmem((max(1, T - 1), part, columns), BF16),
        vmem((part, columns), BF16), vmem((max(1, B - 1), A * R, columns), BF16),
        vmem((A * R, columns), BF16), vmem((max(1, A - 1), R, columns), BF16),
        dma((6,)), dma((T,)), dma((T,)), dma((ep_count,)), dma((ep_count,)),
        dma((T,)), dma((T,)), dma((T,)), dma((T,)),
        dma((NC * T * C,)), dma((NC * T * C,)), dma((NC * T,)), dma((NC * T,)),
        dma((NC * B,)), dma((NC * B,)), dma((NC * A,)), dma((NC * A,)),
    ]
    return pl.pallas_call(
        functools.partial(layer_kernel, n),
        out_shape=jax.ShapeDtypeStruct((R, columns), BF16),
        in_specs=[vm] * 5 + [hbm] * 6,
        out_specs=vm,
        scratch_shapes=scratch,
        compiler_params=pltpu.CompilerParams(
            collective_id=0, has_side_effects=True, vmem_limit_bytes=60 * 1024 * 1024
        ),
    )(
        tokens, head_partial, side, ffn_gain[None, :], branch_gate[None, :],
        expert_gate, expert_up, expert_down, dense_gate, dense_up, dense_down,
    )


def solution(mesh):
    placed = (
        P("ep", None),
        P("ep"),
        P("ep", "tp", None, None),
        P(),
        P(None, "tp"),
        P(None, "tp"),
        P(None, "tp"),
        P("tp", None),
        P(),
        P(),
        P("tp", "ep"),
        P("tp", "ep"),
        P("ep", "tp"),
        P("ep", None),
        P("ep", None),
        P("ep", None, "tp"),
        P("ep", None, "tp"),
        P("ep", "tp", None),
    )
    return jax.shard_map(
        on_device, mesh=mesh, in_specs=placed, out_specs=P("ep", "tp"), check_vma=False
    )
```

time: 170 us -> 57.3 us (0.34)
  waiting for transfers between devices: 74.1 us -> 0 us
  Pallas kernels: 0 us -> 47 us
  blocking collectives: 46 us -> 0 us
  between operations: 13.5 us -> 0.18 us
  matrix products: 16.6 us -> 4.33 us
  starting transfers between devices: 9.31 us -> 0 us
  other arithmetic: 6.78 us -> 3.25 us
    psum x2 -> x0, waiting for transfers between devices: 47.4 us -> none  [the longest x1 24.4 us: on_device(): lax.psum(pre_parts.astype(jnp.float32).astype(jnp.bfloat16), 'tp')]
    pallas_call x0 -> x1, Pallas kernels: none -> 47 us  [on_device(): pl.pallas_call(functools.partial(layer_kernel, n), out_shape=jax.ShapeDty...]
    all_gather x2 -> x0, blocking collectives: 33.9 us -> none  [the longest x1 22.9 us: on_device(): lax.all_gather(own_cols, 'ep', axis=0, tiled=True)]
    all_to_all x2 -> x0, waiting for transfers between devices: 14.8 us -> none  [the longest x1 14.8 us: on_device(): lax.all_to_all(mine, 'ep', split_axis=0, concat_axis=0, tiled=True)]
    all_to_all x1 -> x0, blocking collectives: 12.1 us -> none  [on_device(): lax.all_to_all(blocks_out, 'tp', split_axis=3, concat_axis=3, tiled=True)]
    reduce_scatter x1 -> x0, waiting for transfers between devices: 11.9 us -> none  [on_device(): lax.psum_scatter(jnp.dot(dense_hidden, dense_down, preferred_element_type...]
    dot_general x8 -> x0, matrix products: 11.1 us -> none  [the longest x1 2.29 us: on_device(): jnp.einsum('skcw,kwd->skcd', hidden, expert_down, preferred_element_type=...]
    all_to_all x2 -> x0, starting transfers between devices: 9.19 us -> none  [the longest x1 5.62 us: on_device(): lax.all_to_all(mine, 'ep', split_axis=0, concat_axis=0, tiled=True)]
  transfers between devices with their start and end apart: 5 -> 0, of which waited for: 4 -> 0; matrix products, arithmetic and copies ran while one was open for 6% -> 0% of each run, Pallas kernels for 0% -> 0%
where the time goes in v1:
time: 57.3 us; the launch traced here: 57 us
  Pallas kernels  47 us (82%)
  matrix products  4.33 us (8%)
  other arithmetic  3.25 us (6%)
  local copies, waits for them, and re-layouts  2.3 us (4%)
    pallas_call x1, Pallas kernels, on_device(): pl.pallas_call(functools.partial(layer_kernel, n), out_shape=jax.ShapeDty...  47 us
    dot_general x1, matrix products, on_device(): jnp.dot(normed, w_query, preferred_element_type=jnp.float32)  1.59 us
    dot_general x1, matrix products, on_device(): jnp.dot(normed, w_key, preferred_element_type=jnp.float32)  1.57 us
    unnamed x19, local copies, waits for them, and re-layouts  1.42 us

profile of v1, /device:TPU:0, one launch (start us, length us, event | category | flops | bytes accessed | tf_op | source)
XLA Modules:
  0.0 57.0 jit_solution(10712602577715722681)
XLA Ops:
  0.0 0.0 copy-start
  0.0 0.0 copy-start.8
  0.0 0.0 copy-start.1
  0.0 1.1 %fusion = f32[16]{0:T(128)S(1)} fusion(bf16[16,2048]{1,0:T(8,128)(2,1)} %refs_0_.1), kind=kLoop, calls=%fused_computation.4 | loop fusion | flops 98288 | bytes 65600 | tf_op jit(solution)/shard_map/reduce_sum | solution.py:18
  1.1 0.0 copy-start.2
  1.1 0.0 copy-start.4
  1.2 1.6 %fusion.14 = f32[16,256]{1,0:T(8,128)S(1)} fusion(bf16[2048,256]{1,0:T(8,128)(2,1)} %param.24, bf16[16,2048]{1,0:T(8,128)(2,1)} %refs_0_.1, f32[2048]{0:T(1024)} %param.23, f32[16]{0:T(128)S(1)} %add_rsqrt_fusion.1), kind=kOutput, calls=%fused_computation.36 | convolution fusion | flops 16908288 | bytes 1138752 | tf_op jit(solution)/shard_map/dot_general | solution.py:302
  2.8 1.6 %fusion.12 = f32[16,256]{1,0:T(8,128)S(1)} fusion(bf16[2048,256]{1,0:T(8,128)(2,1)} %param.25, bf16[16,2048]{1,0:T(8,128)(2,1)} %refs_0_.1, f32[2048]{0:T(1024)} %param.23, f32[16]{0:T(128)S(1)} %add_rsqrt_fusion.1), kind=kOutput, calls=%fused_computation.35 | convolution fusion | flops 16908288 | bytes 1138752 | tf_op jit(solution)/shard_map/dot_general | solution.py:305
  4.4 0.0 copy-start.3
  4.4 0.1 fusion.9
  4.5 0.0 copy-done.8
  4.5 0.1 multiply_cosine_fusion
  4.6 0.1 multiply_subtract_fusion.1
  4.7 0.2 fusion.6
  4.9 0.0 copy-done.1
  4.9 0.0 copy-start.5
  4.9 0.0 copy-start.7
  4.9 0.0 copy-start.6
  4.9 0.7 %multiply_reduce_fusion = f32[16,2,128]{2,1,0:T(2,128)S(1)} fusion(f32[16,2,128,128]{3,2,1,0:T(8,128)S(1)} %copy-done.1, f32[16,2,128]{2,1,0:T(2,128)S(1)} %get-tuple-element.7), kind=kLoop, calls=%fused_computation.1 | loop fusion | flops 1044480 | bytes 2129920 | tf_op jit(solution)/shard_map/reduce_sum | solution.py:318
  5.7 0.0 copy-done.2
  5.7 0.0 copy-done.4
  5.7 0.0 copy-done.3
  5.7 0.3 fusion.10
  6.0 0.2 multiply_reduce_fusion.1
  6.2 0.1 mul.218
  6.3 0.1 mul.211
  6.4 0.1 broadcast_bitcast_fusion
  6.4 0.0 copy-done
  6.5 0.9 %convolution_convert_fusion.refs_1_ = bf16[16,2048]{1,0:T(8,128)(2,1)} fusion(bf16[256,2048]{1,0:T(8,128)(2,1)S(1)} %copy-done, f32[2,8,2,128]{3,2,1,0:T(2,128)S(1)} %bitcast.29, f32[16,256]{1,0:T(8,128)S(1)} %fusion.10, f32[2,8,2,128]{3,2,1,0:T(2,128)S(1)} %bitcast.30, f32[2,8,2,128]{3,2,1,0:T(2,128)S(1)} %bitcast.28, f32[256]{0:T(256)S(1)} %broadcast_bitcast_fusion), kind=kOutput, calls=%fused_computation | convolution fusion | flops 16830464 | bytes 1180672 | tf_op jit(solution)/shard_map/dot_general | solution.py:323
  7.3 0.0 copy-done.5
  7.4 0.0 copy-done.7
  7.4 0.7 %select_reduce_fusion.refs_2_ = f32[16,128]{1,0:T(8,128)} fusion(f32[16,6]{0,1:T(8,128)S(1)} %broadcast_divide_fusion, s32[16,6]{0,1:T(8,128)S(1)} %copy-done.7), kind=kLoop, calls=%fused_computation.7 | loop fusion | flops 34816 | bytes 8960 | tf_op jit(solution)/shard_map/reduce_sum | solution.py:336
  8.1 0.0 copy-done.6
  8.1 0.6 %broadcast_in_dim.16.refs_4_ = bf16[1,2048]{1,0:T(2,128)(2,1)} reshape(bf16[2048]{0:T(1024)(128)(2,1)S(1)} %copy-done.6) | data formatting | bytes 8192 | tf_op jit(solution)/shard_map/broadcast_in_dim | solution.py:371
  8.7 47.0 %shard_map.172 = bf16[16,1024]{1,0:T(8,128)(2,1)} custom-call(bf16[16,2048]{1,0:T(8,128)(2,1)} %refs_0_.1, bf16[16,2048]{1,0:T(8,128)(2,1)} %convolution_convert_fusion.refs_1_, f32[16,128]{1,0:T(8,128)} %select_reduce_fusion.refs_2_, f32[1,2048]{1,0:T(1,128)} %bitcast.31, bf16[1,2048]{1,0:T(2,128)(2,1)} %broadcast_in_dim.16.refs_4_, ...), custom_call_target="tpu_custom_call" | custom-call | tf_op jit(solution)/shard_map/pallas_call | solution.py:361
  55.6 1.4 %copy.31 = bf16[16,1024]{1,0:T(8,128)(2,1)} copy(bf16[16,1024]{1,0:T(8,128)(2,1)} %shard_map.172) | data formatting | bytes 65536
  (10 shorter events, 0.1 us)
Async XLA Ops:
  0.0 6.5 %copy-start = (bf16[256,2048]{1,0:T(8,128)(2,1)S(1)}, bf16[256,2048]{1,0:T(8,128)(2,1)}, u32[]{:S(2)}) copy-start(bf16[256,2048]{1,0:T(8,128)(2,1)} %param.27) | copy-start | bytes 3145732
  0.0 4.5 %copy-start.8 = (s32[16]{0:T(128)S(1)}, s32[16]{0:T(128)}, u32[]{:S(2)}) copy-start(s32[16]{0:T(128)} %param.21) | copy-start | bytes 196
  0.0 4.9 %copy-start.1 = (f32[16,2,128,128]{3,2,1,0:T(8,128)S(1)}, f32[16,2,128,128]{3,2,1,0:T(8,128)}, u32[]{:S(2)}) copy-start(f32[16,2,128,128]{3,2,1,0:T(8,128)} %param.22) | copy-start | bytes 6291460
  1.1 4.5 %copy-start.2 = (bf16[16,2048]{1,0:T(8,128)(2,1)S(1)}, bf16[16,2048]{1,0:T(8,128)(2,1)}, u32[]{:S(2)}) copy-start(bf16[16,2048]{1,0:T(8,128)(2,1)} %refs_0_.1) | copy-start | bytes 196612
  1.1 4.5 %copy-start.4 = (f32[2048]{0:T(1024)S(1)}, f32[2048]{0:T(1024)}, u32[]{:S(2)}) copy-start(f32[2048]{0:T(1024)} %param.23) | copy-start | bytes 24580
  4.4 1.3 %copy-start.3 = (bf16[2048,256]{1,0:T(8,128)(2,1)S(1)}, bf16[2048,256]{1,0:T(8,128)(2,1)}, u32[]{:S(2)}) copy-start(bf16[2048,256]{1,0:T(8,128)(2,1)} %param.26) | copy-start | bytes 3145732
  4.9 2.4 %copy-start.5 = (f32[16,6]{0,1:T(8,128)S(1)}, f32[16,6]{0,1:T(8,128)}, u32[]{:S(2)}) copy-start(f32[16,6]{0,1:T(8,128)} %param.34) | copy-start | bytes 1156
  4.9 2.4 %copy-start.7 = (s32[16,6]{0,1:T(8,128)S(1)}, s32[16,6]{0,1:T(8,128)}, u32[]{:S(2)}) copy-start(s32[16,6]{0,1:T(8,128)} %param.33) | copy-start | bytes 1156
  4.9 3.1 %copy-start.6 = (bf16[2048]{0:T(1024)(128)(2,1)S(1)}, bf16[2048]{0:T(1024)(128)(2,1)}, u32[]{:S(2)}) copy-start(bf16[2048]{0:T(1024)(128)(2,1)} %param.29) | copy-start | bytes 12292

commit v2 on v1

v2 whole, which is shorter than its diff:
```python
import functools

import jax
import jax.numpy as jnp
from jax import lax
from jax.experimental import pallas as pl
from jax.experimental.pallas import tpu as pltpu
from jax.sharding import PartitionSpec as P

EPS = 1e-06
MESH = pl.DeviceIdType.MESH
F32 = jnp.float32
BF16 = jnp.bfloat16


def split_ep(count):
    inner = 2 if count % 2 == 0 else 1
    rest = count // inner
    middle = 1
    while middle * middle * 4 <= rest and rest % (middle * 2) == 0:
        middle *= 2
    return rest // middle, middle, inner


class Dims:
    pass


def silu(v):
    return v / (1.0 + jnp.exp(-v))


def layer_kernel(n, *refs):
    (tok, pos, freq, mgain, routes, scores, gain, bgate,
     wq_h, wk_h, wv_h, st_h, wo_h, dg_h, du_h, eg_h, eu_h, ed_h, dd_h, out,
     wq, wk, wv, st, wo, dg, du, eg, eu, ed, dd,
     old, hp, hpr, am, g, pg, pu, s0, rc, s1, rx, s2, ry, s3, rz,
     w_sem, hp_s, hp_r, ag_s, ag_r, pg_s, pg_r, pu_s, pu_r,
     c_s, c_r, x_s, x_r, y_s, y_r, z_s, z_r) = refs
    A, B, C, T, R, D = n.A, n.B, n.C, n.T, n.R, n.D
    cols, S, NC = n.cols, n.S, n.NC
    cw = cols // NC
    ep = lax.axis_index("ep")
    t = lax.axis_index("tp")
    c = lax.rem(ep, C)
    b = lax.rem(lax.div(ep, C), B)
    a = lax.div(ep, B * C)

    def dev(a_, b_, c_):
        return {"ep": (a_ * B + b_) * C + c_}

    def add(i, d, m):
        return lax.rem(i + d, m)

    def slot(a_, b_, c_):
        return (c_ * B + b_) * A + a_

    def rws(s, count=1):
        return pl.ds(pl.multiple_of(s * R, R), count * R)

    names = ("wq", "wk", "wv", "st", "wo", "dg", "du", "eg", "eu", "ed", "dd")
    pairs = ((wq_h, wq), (wk_h, wk), (wv_h, wv), (st_h, st), (wo_h, wo), (dg_h, dg), (du_h, du),
             (eg_h, eg), (eu_h, eu), (ed_h, ed), (dd_h, dd))
    loads = {name: pltpu.make_async_copy(src, dst, w_sem.at[i])
             for i, (name, (src, dst)) in enumerate(zip(names, pairs))}
    for name in names[:5]:
        loads[name].start()

    bar = pltpu.get_barrier_semaphore()
    peers = [dev(add(a, d, A), b, c) for d in range(1, A)]
    peers += [dev(a, add(b, d, B), c) for d in range(1, B)]
    peers += [dev(a, b, add(c, d, C)) for d in range(1, C)]
    peers += [{"tp": add(t, d, T)} for d in range(1, T)]
    for peer in peers:
        pl.semaphore_signal(bar, inc=1, device_id=peer, device_id_type=MESH)

    sent = []

    def push(src, dst, ss, rs, where):
        copy = pltpu.make_async_remote_copy(
            src_ref=src, dst_ref=dst, send_sem=ss, recv_sem=rs, device_id=where, device_id_type=MESH
        )
        copy.start()
        sent.append(copy)

    def arrived(dst, rs):
        pltpu.make_async_remote_copy(
            src_ref=dst, dst_ref=dst, send_sem=rs, recv_sem=rs, device_id={"tp": t}, device_id_type=MESH
        ).wait_recv()

    LH, HD = n.LH, n.HD
    tokens = tok[...].astype(F32)
    normed = (tokens * lax.rsqrt(jnp.mean(tokens * tokens, axis=-1, keepdims=True) + EPS)
              * mgain[...]).astype(BF16)
    angle = pos[...].astype(F32) * freq[...]
    cosine = jnp.cos(angle)
    sine = jnp.sin(angle)
    sine = jnp.where(lax.broadcasted_iota(jnp.int32, (R, HD), 1) < HD // 2, -sine, sine)

    def turn(v):
        return v * cosine + pltpu.roll(v, HD // 2, 1) * sine

    def heads(ref):
        full = jnp.dot(normed, ref[...], preferred_element_type=F32)
        return [full[:, h * HD:(h + 1) * HD] for h in range(LH)]

    loads["wq"].wait()
    query = [turn(v) for v in heads(wq)]
    loads["wk"].wait()
    key = [turn(v) * HD ** (-0.5) for v in heads(wk)]
    loads["wv"].wait()
    value = heads(wv)
    for name in names[5:]:
        loads[name].start()
    loads["st"].wait()
    retrieved = []
    for h in range(LH):
        turned = query[h].T
        for i in range(R):
            old[i:i + 1, h * HD:(h + 1) * HD] = jnp.sum(turned[:, i:i + 1] * st[i, h], axis=0, keepdims=True)
        index = jnp.full((1, HD), t * LH + h, jnp.int32).astype(F32)
        decay = 1.0 - jnp.exp2(-5.0 - 5.0 * index / (LH * T - 1))
        inner = jnp.sum(query[h] * key[h], axis=-1, keepdims=True)
        ret = decay * old[:, h * HD:(h + 1) * HD] + inner * value[h]
        ret = ret * lax.rsqrt(jnp.mean(ret * ret, axis=-1, keepdims=True) + EPS)
        retrieved.append(ret.astype(BF16))
    loads["wo"].wait()
    hp[...] = jnp.dot(jnp.concatenate(retrieved, axis=1), wo[...], preferred_element_type=F32).astype(BF16)
    pl.semaphore_wait(bar, len(peers))

    for d in range(1, T):
        push(hp, hpr.at[d - 1], hp_s.at[d - 1], hp_r.at[d - 1], {"tp": add(t, d, T)})

    lane = lax.broadcasted_iota(jnp.int32, (R, S), 1)
    lane_of = lane % (S // 2)
    marks = scores[...]
    marks = marks / jnp.sum(marks, axis=1, keepdims=True)
    sides = jnp.zeros((R, S), F32)
    for j in range(n.F):
        sides = sides + jnp.where(lane_of == routes[:, j:j + 1], marks[:, j:j + 1], 0.0)

    mixed = hp[...].astype(F32)
    for d in range(1, T):
        arrived(hpr.at[d - 1], hp_r.at[d - 1])
        mixed = mixed + hpr[d - 1].astype(F32)
    after = tokens + mixed
    am[...] = after
    ffn = (after * lax.rsqrt(jnp.mean(after * after, axis=-1, keepdims=True) + EPS) * gain[...]).astype(BF16)
    score = jnp.sum(ffn.astype(F32) * bgate[...].astype(F32), axis=-1, keepdims=True)
    branch = 1.0 / (1.0 + jnp.exp(-score))
    sides = jnp.where(lane_of == n.E, branch, sides)
    high = sides.astype(BF16).astype(F32)
    mine = rws(slot(a, b, c))
    g[mine, 0:D] = ffn
    g[mine, D:D + S] = jnp.where(lane < S // 2, high, sides - high).astype(BF16)

    count = 0
    for da in range(1, A):
        push(g.at[mine], g.at[mine], ag_s.at[count], ag_r.at[slot(a, b, c)], dev(add(a, da, A), b, c))
        count += 1
    for da in range(A):
        aa = add(a, da, A)
        own = rws(slot(aa, b, c))
        if da > 0:
            arrived(g.at[own], ag_r.at[slot(aa, b, c)])
        for db in range(1, B):
            push(g.at[own], g.at[own], ag_s.at[count], ag_r.at[slot(aa, b, c)], dev(a, add(b, db, B), c))
            count += 1
        for dc in range(1, C):
            push(g.at[own], g.at[own], ag_s.at[count], ag_r.at[slot(aa, b, c)], dev(a, b, add(c, dc, C)))
            count += 1

    K = n.K
    GR = A * R
    own_cols = pl.ds(pl.multiple_of(t * cols, 128), cols)
    groups = [(db, dc) for dc in range(C) for db in range(B)]
    hid, wgt, brw, dense = {}, {}, {}, {}

    def group_rows(q):
        return rws(slot(0, add(b, groups[q][0], B), add(c, groups[q][1], C)), A)

    def dense_pre(q):
        gr = group_rows(q)
        x = g[gr, own_cols]
        pg[0, gr, :] = jnp.dot(x, dg[...], preferred_element_type=F32).astype(BF16)
        pu[0, gr, :] = jnp.dot(x, du[...], preferred_element_type=F32).astype(BF16)
        for d in range(1, T):
            i = q * (T - 1) + d - 1
            push(pg.at[0, gr], pg.at[d, gr], pg_s.at[i], pg_r.at[i], {"tp": add(t, d, T)})
            push(pu.at[0, gr], pu.at[d, gr], pu_s.at[i], pu_r.at[i], {"tp": add(t, d, T)})

    def expert_hidden(q):
        gr = group_rows(q)
        sd = g[gr, D:D + S].astype(F32)
        lanes = lax.broadcasted_iota(jnp.int32, (GR, S), 1) % (S // 2)
        brw[q] = jnp.sum(jnp.where(lanes == n.E, sd, 0.0), axis=1, keepdims=True)
        x = g[gr, 0:D]
        for k in range(K):
            gate = jnp.dot(x, eg[k], preferred_element_type=F32)
            up = jnp.dot(x, eu[k], preferred_element_type=F32)
            hid[q, k] = (silu(gate) * up).astype(BF16)
            wgt[q, k] = jnp.sum(jnp.where(lanes == ep * K + k, sd, 0.0), axis=1, keepdims=True)

    def inner_arrived(db, dc):
        for da in range(A):
            ss = slot(add(a, da, A), add(b, db, B), add(c, dc, C))
            arrived(g.at[rws(ss)], ag_r.at[ss])

    for name in ("dg", "du", "eg", "eu"):
        loads[name].wait()
    dense_pre(0)
    expert_hidden(0)
    for db in range(1, B):
        for da in range(A):
            aa, bb = add(a, da, A), add(b, db, B)
            own = rws(slot(aa, bb, c))
            arrived(g.at[own], ag_r.at[slot(aa, bb, c)])
            for dc in range(1, C):
                push(g.at[own], g.at[own], ag_s.at[count], ag_r.at[slot(aa, bb, c)], dev(a, b, add(c, dc, C)))
                count += 1
        dense_pre(db)
    for dc in range(1, C):
        for db in range(B):
            inner_arrived(db, dc)
            dense_pre(dc * B + db)
    for q in range(1, len(groups)):
        expert_hidden(q)
    loads["ed"].wait()
    loads["dd"].wait()

    per_c, per_b = A * B, A

    def chunk(k):
        return slice(k * cw, (k + 1) * cw)

    def stage0(k, dt):
        start = pl.multiple_of(add(t, dt, T) * cols + k * cw, 128)
        order = sorted(range(len(groups)), key=lambda q: -groups[q][1])
        for q in order:
            total = jnp.zeros((GR, cw), F32)
            for e in range(K):
                total = total + wgt[q, e] * jnp.dot(hid[q, e], ed[e, :, pl.ds(start, cw)], preferred_element_type=F32)
            if dt == 0:
                total = total + brw[q] * jnp.dot(dense[q], dd[:, chunk(k)], preferred_element_type=F32)
            s0[dt, group_rows(q), chunk(k)] = total.astype(BF16)
        for dc in range(1, C):
            cc = add(c, dc, C)
            i = (k * T + dt) * (C - 1) + dc - 1
            push(s0.at[dt, rws(cc * per_c, per_c), chunk(k)], rc.at[dc - 1, dt, :, chunk(k)],
                 c_s.at[i], c_r.at[i], dev(a, b, cc))

    def stage1(k, dt):
        acc = s0[dt, rws(c * per_c, per_c), chunk(k)].astype(F32)
        for dc in range(1, C):
            i = (k * T + dt) * (C - 1) + dc - 1
            arrived(rc.at[dc - 1, dt, :, chunk(k)], c_r.at[i])
            acc = acc + rc[dc - 1, dt, :, chunk(k)].astype(F32)
        s1[dt, :, chunk(k)] = acc.astype(BF16)
        if dt > 0:
            i = k * (T - 1) + dt - 1
            push(s1.at[dt, :, chunk(k)], rx.at[dt - 1, :, chunk(k)], x_s.at[i], x_r.at[i], {"tp": add(t, dt, T)})

    def stage2(k):
        acc = s1[0, :, chunk(k)].astype(F32)
        for dt in range(1, T):
            i = k * (T - 1) + dt - 1
            arrived(rx.at[dt - 1, :, chunk(k)], x_r.at[i])
            acc = acc + rx[dt - 1, :, chunk(k)].astype(F32)
        s2[:, chunk(k)] = acc.astype(BF16)
        for db in range(1, B):
            bb = add(b, db, B)
            i = k * (B - 1) + db - 1
            push(s2.at[rws(bb * per_b, per_b), chunk(k)], ry.at[db - 1, :, chunk(k)], y_s.at[i], y_r.at[i], dev(a, bb, c))

    def stage3(k):
        acc = s2[rws(b * per_b, per_b), chunk(k)].astype(F32)
        for db in range(1, B):
            i = k * (B - 1) + db - 1
            arrived(ry.at[db - 1, :, chunk(k)], y_r.at[i])
            acc = acc + ry[db - 1, :, chunk(k)].astype(F32)
        s3[:, chunk(k)] = acc.astype(BF16)
        for da in range(1, A):
            aa = add(a, da, A)
            i = k * (A - 1) + da - 1
            push(s3.at[rws(aa), chunk(k)], rz.at[da - 1, :, chunk(k)], z_s.at[i], z_r.at[i], dev(aa, b, c))

    def stage4(k):
        acc = s3[rws(a), chunk(k)].astype(F32)
        for da in range(1, A):
            i = k * (A - 1) + da - 1
            arrived(rz.at[da - 1, :, chunk(k)], z_r.at[i])
            acc = acc + rz[da - 1, :, chunk(k)].astype(F32)
        base = am[:, pl.ds(pl.multiple_of(t * cols + k * cw, 128), cw)]
        out[:, chunk(k)] = (base + acc).astype(BF16)

    def dense_hidden():
        for q in range(len(groups)):
            gr = group_rows(q)
            for d in range(1, T):
                i = q * (T - 1) + d - 1
                arrived(pg.at[d, gr], pg_r.at[i])
                arrived(pu.at[d, gr], pu_r.at[i])
            pre_g, pre_u = pg[0, gr, :].astype(F32), pu[0, gr, :].astype(F32)
            for d in range(1, T):
                pre_g = pre_g + pg[d, gr, :].astype(F32)
                pre_u = pre_u + pu[d, gr, :].astype(F32)
            dense[q] = (silu(pre_g) * pre_u).astype(BF16)

    far = [(k, dt) for k in range(NC) for dt in range(1, T)]
    for i, item in enumerate(far):
        stage0(*item)
        if i > 0:
            stage1(*far[i - 1])
    dense_hidden()
    if far:
        stage1(*far[-1])
    stages = (lambda k: stage0(k, 0), lambda k: stage1(k, 0), stage2, stage3, stage4)
    for step in range(NC + len(stages) - 1):
        for s, stage in enumerate(stages):
            if 0 <= step - s < NC:
                stage(step - s)

    for copy in sent:
        copy.wait_send()


def on_device(
    tokens,
    positions,
    state,
    mix_gain,
    w_query,
    w_key,
    w_value,
    w_out,
    ffn_gain,
    branch_gate,
    dense_gate,
    dense_up,
    dense_down,
    routes,
    route_scores,
    expert_gate,
    expert_up,
    expert_down,
):
    n = Dims()
    T, ep_count = lax.axis_size("tp"), lax.axis_size("ep")
    A, B, C = split_ep(ep_count)
    R, D = tokens.shape
    columns = D // T
    n.A, n.B, n.C, n.T, n.R, n.D, n.cols = A, B, C, T, R, D, columns
    n.LH, n.HD = state.shape[1], state.shape[2]
    n.F = routes.shape[1]
    n.K = expert_gate.shape[0]
    n.E = n.K * ep_count
    n.S = -(-2 * (n.E + 1) // 128) * 128
    NC = n.NC = columns // 256 if columns % 256 == 0 else 1
    rows = ep_count * R
    hidden = dense_gate.shape[1]
    half = n.HD // 2
    inverse = 1.0 / 10000.0 ** jnp.linspace(0.0, 1.0, half, dtype=jnp.float32)
    freq = jnp.concatenate([inverse, inverse])[None, :]
    vm = pl.BlockSpec(memory_space=pltpu.VMEM)
    hbm = pl.BlockSpec(memory_space=pl.ANY)
    dma = pltpu.SemaphoreType.DMA
    vmem = pltpu.VMEM
    part = A * B * R
    held = [w_query, w_key, w_value, state, w_out, dense_gate, dense_up,
            expert_gate, expert_up, expert_down, dense_down]
    scratch = [vmem(w.shape, w.dtype) for w in held] + [
        vmem((R, n.LH * n.HD), F32), vmem((R, D), BF16),
        vmem((max(1, T - 1), R, D), BF16), vmem((R, D), F32),
        vmem((rows, D + n.S), BF16),
        vmem((T, rows, hidden), BF16), vmem((T, rows, hidden), BF16),
        vmem((T, rows, columns), BF16), vmem((max(1, C - 1), T, part, columns), BF16),
        vmem((T, part, columns), BF16), vmem((max(1, T - 1), part, columns), BF16),
        vmem((part, columns), BF16), vmem((max(1, B - 1), A * R, columns), BF16),
        vmem((A * R, columns), BF16), vmem((max(1, A - 1), R, columns), BF16),
        dma((len(held),)), dma((T,)), dma((T,)), dma((ep_count,)), dma((ep_count,)),
        dma((B * C * T,)), dma((B * C * T,)), dma((B * C * T,)), dma((B * C * T,)),
        dma((NC * T * C,)), dma((NC * T * C,)), dma((NC * T,)), dma((NC * T,)),
        dma((NC * B,)), dma((NC * B,)), dma((NC * A,)), dma((NC * A,)),
    ]
    return pl.pallas_call(
        functools.partial(layer_kernel, n),
        out_shape=jax.ShapeDtypeStruct((R, columns), BF16),
        in_specs=[vm] * 8 + [hbm] * len(held),
        out_specs=vm,
        scratch_shapes=scratch,
        compiler_params=pltpu.CompilerParams(
            collective_id=0, has_side_effects=True, vmem_limit_bytes=60 * 1024 * 1024
        ),
    )(
        tokens, positions[:, None], freq, mix_gain[None, :], routes, route_scores,
        ffn_gain[None, :], branch_gate[None, :], *held,
    )


def solution(mesh):
    placed = (
        P("ep", None),
        P("ep"),
        P("ep", "tp", None, None),
        P(),
        P(None, "tp"),
        P(None, "tp"),
        P(None, "tp"),
        P("tp", None),
        P(),
        P(),
        P("tp", "ep"),
        P("tp", "ep"),
        P("ep", "tp"),
        P("ep", None),
        P("ep", None),
        P("ep", None, "tp"),
        P("ep", None, "tp"),
        P("ep", "tp", None),
    )
    return jax.shard_map(
        on_device, mesh=mesh, in_specs=placed, out_specs=P("ep", "tp"), check_vma=False
    )
```

time: 57.3 us -> 53.9 us (0.941)
  local copies, waits for them, and re-layouts: 2.3 us -> 6.7 us
  matrix products: 4.33 us -> 0 us
  other arithmetic: 3.25 us -> 0.69 us
  Pallas kernels: 47 us -> 46.2 us
    dot_general x4 -> x0, matrix products: 4.33 us -> none  [the longest x1 1.59 us: on_device(): jnp.dot(normed, w_query, preferred_element_type=jnp.float32)]
    reduce_sum x6 -> x0, other arithmetic: 2.9 us -> none  [the longest x1 1.12 us: normalize(): jnp.mean(values * values, axis=-1, keepdims=True) + EPS]
    unnamed x19 -> x3, local copies, waits for them, and re-layouts: 1.42 us -> 4.09 us
    broadcast_in_dim x0 -> x1, local copies, waits for them, and re-layouts: none -> 1.33 us  [on_device(): positions[:, None]]
    pallas_call x1, Pallas kernels: 47 us -> 46.2 us  [on_device(): pl.pallas_call(functools.partial(layer_kernel, n), out_shape=jax.ShapeDty...]
    broadcast_in_dim x1, local copies, waits for them, and re-layouts: 0.6 us -> 1.28 us  [on_device(): branch_gate[None, :]]
    broadcast_in_dim x0 -> x1, other arithmetic: none -> 0.6 us  [on_device(): freq = jnp.concatenate([inverse, inverse])[None, :]]
where the time goes in v2:
time: 53.9 us; the launch traced here: 53.6 us
  Pallas kernels  46.2 us (86%)
  local copies, waits for them, and re-layouts  6.7 us (12%)
  other arithmetic  0.69 us (1%)
    pallas_call x1, Pallas kernels, on_device(): pl.pallas_call(functools.partial(layer_kernel, n), out_shape=jax.ShapeDty...  46.2 us
    unnamed x3, local copies, waits for them, and re-layouts  4.09 us
    broadcast_in_dim x1, local copies, waits for them, and re-layouts, on_device(): positions[:, None]  1.33 us
    broadcast_in_dim x1, local copies, waits for them, and re-layouts, on_device(): branch_gate[None, :]  1.28 us

profile of v2, /device:TPU:0, one launch (start us, length us, event | category | flops | bytes accessed | tf_op | source)
XLA Modules:
  0.0 53.6 jit_solution(14361748451475494532)
XLA Ops:
  0.0 0.1 fusion
  0.1 0.6 %maximum_bitcast_fusion.refs_2_ = f32[1,128]{1,0:T(1,128)} fusion(f32[64]{0:T(128)S(1)} %fusion), kind=kLoop, calls=%fused_computation.2 | loop fusion | flops 128 | bytes 768 | tf_op jit(solution)/shard_map/broadcast_in_dim | solution.py:363
  0.7 1.3 %copy.19.refs_1_ = s32[16,1]{1,0:T(8,128)} copy(s32[16,1]{0,1:T(1,128)} %bitcast.7) | data formatting | bytes 128 | tf_op jit(solution)/shard_map/broadcast_in_dim | solution.py:395
  2.0 1.3 %broadcast_in_dim.21.refs_7_ = bf16[1,2048]{1,0:T(2,128)(2,1)} reshape(bf16[2048]{0:T(1024)(128)(2,1)} %param.27) | data formatting | bytes 8192 | tf_op jit(solution)/shard_map/broadcast_in_dim | solution.py:396
  3.3 1.4 %copy.20.refs_4_ = s32[16,6]{1,0:T(8,128)} copy(s32[16,6]{0,1:T(8,128)} %param.31) | data formatting | bytes 768 | tf_op args[13]
  4.7 1.4 %copy.21.refs_5_ = f32[16,6]{1,0:T(8,128)} copy(f32[16,6]{0,1:T(8,128)} %param.32) | data formatting | bytes 768 | tf_op args[14]
  6.0 46.2 %shard_map.172 = bf16[16,1024]{1,0:T(8,128)(2,1)} custom-call(bf16[16,2048]{1,0:T(8,128)(2,1)} %refs_0_.1, s32[16,1]{1,0:T(8,128)} %copy.19.refs_1_, f32[1,128]{1,0:T(1,128)} %maximum_bitcast_fusion.refs_2_, f32[1,2048]{1,0:T(1,128)} %bitcast.5, s32[16,6]{1,0:T(8,128)} %copy.20.refs_4_, f32[16,6]{1,0:T(8,128)} %copy.21.refs_5_, f32[1,2048]{1,0:T(1,128)} %bitcast.6, ...), custom_call_target="tpu_custom_call" | custom-call | tf_op jit(solution)/shard_map/pallas_call | solution.py:385
  52.2 1.4 %copy.23 = bf16[16,1024]{1,0:T(8,128)(2,1)} copy(bf16[16,1024]{1,0:T(8,128)(2,1)} %shard_map.172) | data formatting | bytes 65536
  (1 shorter events, 0.0 us)

commit v3 on v2

--- a/solution.py
+++ b/solution.py
@@ -2,6 +2,7 @@
 
 import jax
 import jax.numpy as jnp
+import numpy as np
 from jax import lax
 from jax.experimental import pallas as pl
 from jax.experimental.pallas import tpu as pltpu
@@ -92,7 +93,12 @@
     tokens = tok[...].astype(F32)
     normed = (tokens * lax.rsqrt(jnp.mean(tokens * tokens, axis=-1, keepdims=True) + EPS)
               * mgain[...]).astype(BF16)
-    angle = pos[...].astype(F32) * freq[...]
+    eye = lax.broadcasted_iota(jnp.int32, (R, R), 0) == lax.broadcasted_iota(jnp.int32, (R, R), 1)
+
+    def column(row):
+        return jnp.sum(jnp.where(eye, row.astype(F32), 0.0), axis=1, keepdims=True)
+
+    angle = column(pos[...]) * freq[...]
     cosine = jnp.cos(angle)
     sine = jnp.sin(angle)
     sine = jnp.where(lax.broadcasted_iota(jnp.int32, (R, HD), 1) < HD // 2, -sine, sine)
@@ -133,11 +139,12 @@
 
     lane = lax.broadcasted_iota(jnp.int32, (R, S), 1)
     lane_of = lane % (S // 2)
-    marks = scores[...]
-    marks = marks / jnp.sum(marks, axis=1, keepdims=True)
+    shares = scores[...]
+    shares = shares / jnp.sum(shares, axis=0, keepdims=True)
+    chosen = routes[...]
     sides = jnp.zeros((R, S), F32)
     for j in range(n.F):
-        sides = sides + jnp.where(lane_of == routes[:, j:j + 1], marks[:, j:j + 1], 0.0)
+        sides = sides + jnp.where(lane_of.astype(F32) == column(chosen[j:j + 1]), column(shares[j:j + 1]), 0.0)
 
     mixed = hp[...].astype(F32)
     for d in range(1, T):
@@ -146,7 +153,10 @@
     after = tokens + mixed
     am[...] = after
     ffn = (after * lax.rsqrt(jnp.mean(after * after, axis=-1, keepdims=True) + EPS) * gain[...]).astype(BF16)
-    score = jnp.sum(ffn.astype(F32) * bgate[...].astype(F32), axis=-1, keepdims=True)
+    score = jnp.zeros((R, 128), F32)
+    for j in range(D // 128):
+        score = score + ffn[:, j * 128:(j + 1) * 128].astype(F32) * bgate[j:j + 1, :].astype(F32)
+    score = jnp.sum(score, axis=-1, keepdims=True)
     branch = 1.0 / (1.0 + jnp.exp(-score))
     sides = jnp.where(lane_of == n.E, branch, sides)
     high = sides.astype(BF16).astype(F32)
@@ -219,11 +229,12 @@
                 push(g.at[own], g.at[own], ag_s.at[count], ag_r.at[slot(aa, bb, c)], dev(a, b, add(c, dc, C)))
                 count += 1
         dense_pre(db)
+        expert_hidden(db)
     for dc in range(1, C):
         for db in range(B):
             inner_arrived(db, dc)
             dense_pre(dc * B + db)
-    for q in range(1, len(groups)):
+    for q in range(B, len(groups)):
         expert_hidden(q)
     loads["ed"].wait()
     loads["dd"].wait()
@@ -242,54 +253,54 @@
                 total = total + wgt[q, e] * jnp.dot(hid[q, e], ed[e, :, pl.ds(start, cw)], preferred_element_type=F32)
             if dt == 0:
                 total = total + brw[q] * jnp.dot(dense[q], dd[:, chunk(k)], preferred_element_type=F32)
-            s0[dt, group_rows(q), chunk(k)] = total.astype(BF16)
+            s0[k, dt, group_rows(q)] = total.astype(BF16)
         for dc in range(1, C):
             cc = add(c, dc, C)
             i = (k * T + dt) * (C - 1) + dc - 1
-            push(s0.at[dt, rws(cc * per_c, per_c), chunk(k)], rc.at[dc - 1, dt, :, chunk(k)],
+            push(s0.at[k, dt, rws(cc * per_c, per_c)], rc.at[k, dc - 1, dt],
                  c_s.at[i], c_r.at[i], dev(a, b, cc))
 
     def stage1(k, dt):
-        acc = s0[dt, rws(c * per_c, per_c), chunk(k)].astype(F32)
+        acc = s0[k, dt, rws(c * per_c, per_c)].astype(F32)
         for dc in range(1, C):
             i = (k * T + dt) * (C - 1) + dc - 1
-            arrived(rc.at[dc - 1, dt, :, chunk(k)], c_r.at[i])
-            acc = acc + rc[dc - 1, dt, :, chunk(k)].astype(F32)
-        s1[dt, :, chunk(k)] = acc.astype(BF16)
+            arrived(rc.at[k, dc - 1, dt], c_r.at[i])
+            acc = acc + rc[k, dc - 1, dt].astype(F32)
+        s1[k, dt] = acc.astype(BF16)
         if dt > 0:
             i = k * (T - 1) + dt - 1
-            push(s1.at[dt, :, chunk(k)], rx.at[dt - 1, :, chunk(k)], x_s.at[i], x_r.at[i], {"tp": add(t, dt, T)})
+            push(s1.at[k, dt], rx.at[k, dt - 1], x_s.at[i], x_r.at[i], {"tp": add(t, dt, T)})
 
     def stage2(k):
-        acc = s1[0, :, chunk(k)].astype(F32)
+        acc = s1[k, 0].astype(F32)
         for dt in range(1, T):
             i = k * (T - 1) + dt - 1
-            arrived(rx.at[dt - 1, :, chunk(k)], x_r.at[i])
-            acc = acc + rx[dt - 1, :, chunk(k)].astype(F32)
-        s2[:, chunk(k)] = acc.astype(BF16)
+            arrived(rx.at[k, dt - 1], x_r.at[i])
+            acc = acc + rx[k, dt - 1].astype(F32)
+        s2[k] = acc.astype(BF16)
         for db in range(1, B):
             bb = add(b, db, B)
             i = k * (B - 1) + db - 1
-            push(s2.at[rws(bb * per_b, per_b), chunk(k)], ry.at[db - 1, :, chunk(k)], y_s.at[i], y_r.at[i], dev(a, bb, c))
+            push(s2.at[k, rws(bb * per_b, per_b)], ry.at[k, db - 1], y_s.at[i], y_r.at[i], dev(a, bb, c))
 
     def stage3(k):
-        acc = s2[rws(b * per_b, per_b), chunk(k)].astype(F32)
+        acc = s2[k, rws(b * per_b, per_b)].astype(F32)
         for db in range(1, B):
             i = k * (B - 1) + db - 1
-            arrived(ry.at[db - 1, :, chunk(k)], y_r.at[i])
-            acc = acc + ry[db - 1, :, chunk(k)].astype(F32)
-        s3[:, chunk(k)] = acc.astype(BF16)
+            arrived(ry.at[k, db - 1], y_r.at[i])
+            acc = acc + ry[k, db - 1].astype(F32)
+        s3[k] = acc.astype(BF16)
         for da in range(1, A):
             aa = add(a, da, A)
             i = k * (A - 1) + da - 1
-            push(s3.at[rws(aa), chunk(k)], rz.at[da - 1, :, chunk(k)], z_s.at[i], z_r.at[i], dev(aa, b, c))
+            push(s3.at[k, rws(aa)], rz.at[k, da - 1], z_s.at[i], z_r.at[i], dev(aa, b, c))
 
     def stage4(k):
-        acc = s3[rws(a), chunk(k)].astype(F32)
+        acc = s3[k, rws(a)].astype(F32)
         for da in range(1, A):
             i = k * (A - 1) + da - 1
-            arrived(rz.at[da - 1, :, chunk(k)], z_r.at[i])
-            acc = acc + rz[da - 1, :, chunk(k)].astype(F32)
+            arrived(rz.at[k, da - 1], z_r.at[i])
+            acc = acc + rz[k, da - 1].astype(F32)
         base = am[:, pl.ds(pl.multiple_of(t * cols + k * cw, 128), cw)]
         out[:, chunk(k)] = (base + acc).astype(BF16)
 
@@ -355,12 +366,13 @@
     n.K = expert_gate.shape[0]
     n.E = n.K * ep_count
     n.S = -(-2 * (n.E + 1) // 128) * 128
-    NC = n.NC = columns // 256 if columns % 256 == 0 else 1
+    NC = n.NC = columns // 512 if columns % 512 == 0 else 1
+    wide = columns // NC
     rows = ep_count * R
     hidden = dense_gate.shape[1]
     half = n.HD // 2
-    inverse = 1.0 / 10000.0 ** jnp.linspace(0.0, 1.0, half, dtype=jnp.float32)
-    freq = jnp.concatenate([inverse, inverse])[None, :]
+    inverse = 1.0 / 10000.0 ** (np.arange(half) / (half - 1))
+    freq = np.concatenate([inverse, inverse])[None, :].astype(np.float32)
     vm = pl.BlockSpec(memory_space=pltpu.VMEM)
     hbm = pl.BlockSpec(memory_space=pl.ANY)
     dma = pltpu.SemaphoreType.DMA
@@ -373,10 +385,10 @@
         vmem((max(1, T - 1), R, D), BF16), vmem((R, D), F32),
         vmem((rows, D + n.S), BF16),
         vmem((T, rows, hidden), BF16), vmem((T, rows, hidden), BF16),
-        vmem((T, rows, columns), BF16), vmem((max(1, C - 1), T, part, columns), BF16),
-        vmem((T, part, columns), BF16), vmem((max(1, T - 1), part, columns), BF16),
-        vmem((part, columns), BF16), vmem((max(1, B - 1), A * R, columns), BF16),
-        vmem((A * R, columns), BF16), vmem((max(1, A - 1), R, columns), BF16),
+        vmem((NC, T, rows, wide), BF16), vmem((NC, max(1, C - 1), T, part, wide), BF16),
+        vmem((NC, T, part, wide), BF16), vmem((NC, max(1, T - 1), part, wide), BF16),
+        vmem((NC, part, wide), BF16), vmem((NC, max(1, B - 1), A * R, wide), BF16),
+        vmem((NC, A * R, wide), BF16), vmem((NC, max(1, A - 1), R, wide), BF16),
         dma((len(held),)), dma((T,)), dma((T,)), dma((ep_count,)), dma((ep_count,)),
         dma((B * C * T,)), dma((B * C * T,)), dma((B * C * T,)), dma((B * C * T,)),
         dma((NC * T * C,)), dma((NC * T * C,)), dma((NC * T,)), dma((NC * T,)),
@@ -392,8 +404,8 @@
             collective_id=0, has_side_effects=True, vmem_limit_bytes=60 * 1024 * 1024
         ),
     )(
-        tokens, positions[:, None], freq, mix_gain[None, :], routes, route_scores,
-        ffn_gain[None, :], branch_gate[None, :], *held,
+        tokens, positions[None, :], freq, mix_gain[None, :], routes.T, route_scores.T,
+        ffn_gain[None, :], branch_gate.reshape(D // 128, 128), *held,
     )
 
 

time: 53.9 us -> 44.1 us (0.82)
  local copies, waits for them, and re-layouts: 6.7 us -> 1.38 us
  Pallas kernels: 46.2 us -> 42.5 us
  other arithmetic: 0.69 us -> 0 us
    pallas_call x1, Pallas kernels: 46.2 us -> 42.5 us  [on_device(): pl.pallas_call(functools.partial(layer_kernel, n), out_shape=jax.ShapeDty...]
    unnamed x3 -> x1, local copies, waits for them, and re-layouts: 4.09 us -> 1.38 us
    broadcast_in_dim x2 -> x0, local copies, waits for them, and re-layouts: 2.61 us -> none  [the longest x1 1.33 us: on_device(): positions[:, None]]
    broadcast_in_dim x1 -> x0, other arithmetic: 0.6 us -> none  [on_device(): freq = jnp.concatenate([inverse, inverse])[None, :]]
where the time goes in v3:
time: 44.1 us; the launch traced here: 43.9 us
  Pallas kernels  42.5 us (96%)
  local copies, waits for them, and re-layouts  1.38 us (3%)
    pallas_call x1, Pallas kernels, on_device(): pl.pallas_call(functools.partial(layer_kernel, n), out_shape=jax.ShapeDty...  42.5 us
    unnamed x1, local copies, waits for them, and re-layouts  1.38 us

profile of v3, /device:TPU:0, one launch (start us, length us, event | category | flops | bytes accessed | tf_op | source)
XLA Modules:
  0.0 43.9 jit_solution(11838451013138647009)
XLA Ops:
  0.0 42.5 %shard_map.181 = bf16[16,1024]{1,0:T(8,128)(2,1)} custom-call(bf16[16,2048]{1,0:T(8,128)(2,1)} %refs_0_.1, s32[1,16]{1,0:T(1,128)} %bitcast.11, f32[1,128]{1,0:T(1,128)} %constant.2.clone.refs_2_, f32[1,2048]{1,0:T(1,128)} %bitcast.6, s32[6,16]{1,0:T(8,128)} %bitcast.8, f32[6,16]{1,0:T(8,128)} %bitcast.9, f32[1,2048]{1,0:T(1,128)} %bitcast.7, ...), custom_call_target="tpu_custom_call" | custom-call | tf_op jit(solution)/shard_map/pallas_call | solution.py:397
  42.5 1.4 %copy.21 = bf16[16,1024]{1,0:T(8,128)(2,1)} copy(bf16[16,1024]{1,0:T(8,128)(2,1)} %shard_map.181) | data formatting | bytes 65536
